TPU v7x, 32 devices: a whole 2x2x4 slice. The times are simulated.
32 devices in a mesh: sp: 4 (over z), fs: 4 (over y, x), tp: 2 (over core).
Axes of the slice: x: 2, y: 2, z: 4, core: 2. Of those that a mesh axis runs over, the one named last changes fastest.
Arguments:
- tokens: bfloat16 [4, 1024, 2048], P('fs', 'sp'), may hold values from -6 to 6
- norm_gain: float32 [2048], replicated, may hold values from 0.1 to 1.9
- pool_input: bfloat16 [2048, 2048], P(('sp', 'fs'), 'tp'), may hold values from -0.125 to 0.125
- query_weight: bfloat16 [2048, 2048], P(('sp', 'fs'), 'tp'), may hold values from -20 to 20
- key_weight: bfloat16 [2048, 2048], P(('sp', 'fs'), 'tp'), may hold values from -1 to 1
- value_weight: bfloat16 [2048, 2048], P(('sp', 'fs'), 'tp'), may hold values from -0.125 to 0.125
- pool_map: bfloat16 [8, 256, 256], P('tp'), may hold values from -0.375 to 0.375
- pool_scale: float32 [2048], P('tp'), may hold values from 0.1 to 1.9
- head_gain: float32 [256], replicated, may hold values from 0.1 to 1.9
- diff_lambda: float32 [8], replicated, may hold values from 0.3 to 0.8
- out_pool: bfloat16 [2048, 2048], P('tp', ('sp', 'fs')), may hold values from -0.09375 to 0.09375
- out_heads: bfloat16 [2048, 2048], P('tp', ('sp', 'fs')), may hold values from -0.09375 to 0.09375
Outputs:
- layer_out: bfloat16 [4, 1024, 2048], P('fs', 'sp', 'tp')
All inputs are finite; a program needn't handle non-finite values.
Results may differ from a plain program's by a relative error of at most 0.018.
Values may be sent and summed in bfloat16 or wider, within the bound.
A program may use at most 64 MiB of HBM per device.

v0:
```python
import math

import jax
import jax.numpy as jnp
from jax import lax
from jax.sharding import PartitionSpec as P

HEAD_DIM = 128
GROUP_DIM = 256


THETA = 500000.0
HEAD_SCALE = 0.8
NORM_EPS = 1e-06
HEAD_EPS = 1e-05


def from_behind(value, axis, steps):
    count = lax.axis_size(axis)
    first, last = (max(0, -steps), min(count, count - steps))
    return lax.ppermute(value, axis, [(source, source + steps) for source in range(first, last)])


def rotate(tensor, positions):
    half = HEAD_DIM // 2
    freqs = 1.0 / THETA ** (jnp.arange(half, dtype=jnp.float32) * 2.0 / HEAD_DIM)
    angles = positions[:, None] * freqs[None, :]
    cosine = jnp.cos(angles)[:, None, None, :]
    sine = jnp.sin(angles)[:, None, None, :]
    floated = tensor.astype(jnp.float32)
    first = floated[..., :half]
    second = floated[..., half:]
    turned = jnp.concatenate([first * cosine - second * sine, second * cosine + first * sine], -1)
    return turned.astype(jnp.bfloat16)


def local(
    tokens,
    norm_gain,
    pool_input,
    query_weight,
    key_weight,
    value_weight,
    pool_map,
    pool_scale,
    head_gain,
    diff_lambda,
    out_pool,
    out_heads,
):
    out_local = jnp.concatenate([out_pool, out_heads], 0)
    row_count = tokens.shape[1]
    floated = tokens[0].astype(jnp.float32)
    normed = (
        floated * lax.rsqrt(jnp.mean(floated * floated, -1, keepdims=True) + NORM_EPS) * norm_gain
    ).astype(jnp.bfloat16)
    fragments = (
        lax.all_gather(pool_input, ("sp", "fs"), axis=0, tiled=True),
        lax.all_gather(query_weight, ("sp", "fs"), axis=0, tiled=True),
        lax.all_gather(key_weight, ("sp", "fs"), axis=0, tiled=True),
        lax.all_gather(value_weight, ("sp", "fs"), axis=0, tiled=True),
    )
    projected = tuple(
        (jnp.dot(normed, fragment, preferred_element_type=jnp.float32) for fragment in fragments)
    )
    pool_in, queries, keys_flat, values_flat = [
        product.astype(jnp.bfloat16) for product in projected
    ]
    head_count = values_flat.shape[1] // (2 * HEAD_DIM)
    tp_index = lax.axis_index("tp")
    sp_index = lax.axis_index("sp")
    query_pos = sp_index * row_count + jnp.arange(row_count, dtype=jnp.int32)
    positions = query_pos.astype(jnp.float32)
    queries = rotate(queries.reshape(row_count, head_count, 2, HEAD_DIM), positions)
    keys_flat = rotate(keys_flat.reshape(row_count, head_count, 2, HEAD_DIM), positions).reshape(
        row_count, head_count * 2 * HEAD_DIM
    )
    lambdas = lax.dynamic_slice_in_dim(diff_lambda, tp_index * head_count, head_count, 0)

    def online_step(state, key_rows, value_rows, key_offset):
        largest, summed, accum = state
        width = key_rows.shape[0]
        shaped = key_rows.reshape(width, head_count, 2, HEAD_DIM)
        scores = jnp.einsum(
            "qhcd,khcd->chqk", queries, shaped, preferred_element_type=jnp.float32
        ) * HEAD_DIM ** (-0.5)
        key_pos = key_offset + jnp.arange(width, dtype=jnp.int32)
        scores = jnp.where(query_pos[:, None] >= key_pos[None, :], scores, -jnp.inf)
        newest = jnp.maximum(largest, jnp.max(scores, -1))
        anchor = jnp.where(jnp.isfinite(newest), newest, 0.0)
        rescale = jnp.exp(largest - anchor)
        expons = jnp.exp(scores - anchor[..., None])
        summed = summed * rescale + jnp.sum(expons, -1)
        value_shaped = value_rows.reshape(width, head_count, 2 * HEAD_DIM)
        added = jnp.einsum(
            "chqk,khe->chqe",
            expons.astype(jnp.bfloat16),
            value_shaped,
            preferred_element_type=jnp.float32,
        )
        accum = accum * rescale[..., None] + added
        return (newest, summed, accum)

    start_state = (
        jnp.full((2, head_count, row_count), -jnp.inf, jnp.float32),
        jnp.zeros((2, head_count, row_count), jnp.float32),
        jnp.zeros((2, head_count, row_count, 2 * HEAD_DIM), jnp.float32),
    )
    fragments = (
        lax.all_gather(keys_flat, "sp", axis=0, tiled=True),
        lax.all_gather(values_flat, "sp", axis=0, tiled=True),
    )
    span = math.gcd(fragments[0].shape[0], 1024)

    def inner_step(index, inner_state):
        key_rows = lax.dynamic_slice_in_dim(fragments[0], index * span, span, 0)
        value_rows = lax.dynamic_slice_in_dim(fragments[1], index * span, span, 0)
        return online_step(inner_state, key_rows, value_rows, index * span)

    final_state = lax.fori_loop(0, fragments[0].shape[0] // span, inner_step, start_state)
    summed_final = final_state[1]
    accum_final = final_state[2]
    heads_raw = (
        accum_final[0] / summed_final[0][..., None]
        - lambdas[:, None, None] * accum_final[1] / summed_final[1][..., None]
    )
    heads_raw = jnp.moveaxis(heads_raw, 0, 1)
    attn = (
        (
            heads_raw
            * lax.rsqrt(jnp.mean(heads_raw * heads_raw, -1, keepdims=True) + HEAD_EPS)
            * head_gain
            * HEAD_SCALE
        )
        .astype(jnp.bfloat16)
        .reshape(row_count, head_count * 2 * HEAD_DIM)
    )
    reach = 15
    rim_rows = from_behind(pool_in[row_count - reach :], "sp", 1)
    extended = jnp.concatenate([rim_rows, pool_in], 0).astype(jnp.float32)
    pair_sums = extended[1:] + extended[:-1]
    quad_sums = pair_sums[2:] + pair_sums[:-2]
    octet_sums = quad_sums[4:] + quad_sums[:-4]
    sixteen_sums = octet_sums[8:] + octet_sums[:-8]
    group_count = pool_in.shape[1] // GROUP_DIM
    stacked = jnp.stack(
        [
            pair_sums[14 : 14 + row_count],
            quad_sums[12 : 12 + row_count],
            octet_sums[8 : 8 + row_count],
            sixteen_sums,
        ],
        0,
    ).reshape(4, row_count, group_count, GROUP_DIM)
    levels = (tp_index * group_count + jnp.arange(group_count, dtype=jnp.int32)) % 4
    picked = jnp.sum(
        jnp.where(
            levels[None, None, :, None] == jnp.arange(4, dtype=jnp.int32)[:, None, None, None],
            stacked,
            0.0,
        ),
        0,
    )
    windows = 2 ** (1 + levels)
    counts = jnp.minimum(query_pos[:, None] + 1, windows[None, :]).astype(jnp.float32)
    window_mean = picked / counts[:, :, None]
    grouped = pool_in.reshape(row_count, group_count, GROUP_DIM).astype(jnp.float32)
    pool_mixed = (window_mean - grouped).astype(jnp.bfloat16)
    pooled = (
        (
            jnp.einsum("tgc,gce->tge", pool_mixed, pool_map, preferred_element_type=jnp.float32)
            * pool_scale.reshape(group_count, GROUP_DIM)
        )
        .astype(jnp.bfloat16)
        .reshape(row_count, group_count * GROUP_DIM)
    )
    branches = jnp.concatenate([pooled, attn], 1)
    partial_value = jnp.dot(
        branches,
        lax.all_gather(out_local, ("sp", "fs"), axis=1, tiled=True),
        preferred_element_type=jnp.float32,
    )
    layer_out = lax.psum_scatter(
        partial_value.astype(jnp.bfloat16), "tp", scatter_dimension=1, tiled=True
    )
    return layer_out[None]


def solution(mesh):
    placed = (
        P("fs", "sp", None),
        P(),
        P(("sp", "fs"), "tp"),
        P(("sp", "fs"), "tp"),
        P(("sp", "fs"), "tp"),
        P(("sp", "fs"), "tp"),
        P("tp", None, None),
        P("tp"),
        P(),
        P(),
        P("tp", ("sp", "fs")),
        P("tp", ("sp", "fs")),
    )
    return jax.shard_map(
        local, mesh=mesh, in_specs=placed, out_specs=P("fs", "sp", "tp"), check_vma=False
    )
```

profile of v0, /device:TPU:10, one launch (start us, length us, event | category | flops | bytes accessed | tf_op | source)
XLA Modules:
  0.0 573.4 jit_solution(961941928835282613)
XLA Ops:
  11.5 75.4 %all-gather.10.cloned.1.call-done = bf16[2048,1024]{1,0:T(8,128)(2,1)} async-done(((bf16[128,1024]{1,0:T(8,128)(2,1)}), bf16[2048,1024]{1,0:T(8,128)(2,1)}) %all-gather.10.cloned.1.call-update) | async-done | bytes 4194320 | tf_op jit(solution)/shard_map/all_gather | solution.py:59
  86.8 4.5 fusion.15
  91.3 2.1 reshape.246
  93.4 70.4 %all-gather.12.cloned.1.call-done = bf16[2048,1024]{1,0:T(8,128)(2,1)} async-done(((bf16[128,1024]{1,0:T(8,128)(2,1)}), bf16[2048,1024]{1,0:T(8,128)(2,1)}) %all-gather.12.cloned.1.call-update) | async-done | bytes 4194320 | tf_op jit(solution)/shard_map/all_gather | solution.py:60
  163.8 4.5 fusion.14
  170.4 2.9 fusion.41
  176.4 64.5 %all-gather.16.cloned.1.call-done = bf16[2048,1024]{1,0:T(8,128)(2,1)} async-done(((bf16[128,1024]{1,0:T(8,128)(2,1)}), bf16[2048,1024]{1,0:T(8,128)(2,1)}) %all-gather.16.cloned.1.call-update) | async-done | bytes 4194320 | tf_op jit(solution)/shard_map/all_gather | solution.py:61
  240.8 4.3 convolution_convert_fusion.1
  246.5 71.2 %all-gather.8.cloned.1.call-done = bf16[2048,1024]{1,0:T(8,128)(2,1)} async-done(((bf16[128,1024]{1,0:T(8,128)(2,1)}), bf16[2048,1024]{1,0:T(8,128)(2,1)}) %all-gather.8.cloned.1.call-update) | async-done | bytes 4194320 | tf_op jit(solution)/shard_map/all_gather | solution.py:58
  317.7 3.5 convolution_convert_fusion.4
  321.2 3.1 collective-permute-start
  330.7 2.7 stack.17
  333.4 2.7 stack.18
  336.1 2.7 stack.16
  340.3 3.2 fusion.3
  345.1 16.2 %all-gather.14.cloned.1.call-done = bf16[1024,1024]{0,1:T(8,128)(2,1)} async-done(((bf16[256,1024]{0,1:T(8,128)(2,1)}), bf16[1024,1024]{0,1:T(8,128)(2,1)}) %all-gather.14.cloned.1.call-update) | async-done | bytes 2097168 | tf_op jit(solution)/shard_map/all_gather | solution.py:110
  361.3 3.6 fusion
  364.8 3.7 fusion.2
  368.5 39.5 %all-gather.18.cloned.1.call-done = bf16[1024,1024]{1,0:T(8,128)(2,1)} async-done(((bf16[256,1024]{1,0:T(8,128)(2,1)}), bf16[1024,1024]{1,0:T(8,128)(2,1)}) %all-gather.18.cloned.1.call-update) | async-done | bytes 2097168 | tf_op jit(solution)/shard_map/all_gather | solution.py:111
  408.0 2.9 copy.64
  410.9 3.5 bitcast_add_fusion
  415.2 134.7 %all-gather.20.cloned.1.call-done = bf16[2048,2048]{1,0:T(8,128)(2,1)} async-done(((bf16[2048,128]{1,0:T(8,128)(2,1)}), bf16[2048,2048]{1,0:T(8,128)(2,1)}) %all-gather.20.cloned.1.call-update) | async-done | bytes 8388624 | tf_op jit(solution)/shard_map/all_gather | solution.py:180
  549.9 6.8 %convolution_convert_fusion = bf16[256,2048]{1,0:T(8,128)(2,1)} fusion(bf16[2048,2048]{1,0:T(8,128)(2,1)} %all-gather.20.cloned.1.call-done, bf16[256,1024]{0,1:T(8,128)(2,1)S(1)} %bitcast.59, bf16[256,1024]{0,1:T(8,128)(2,1)S(1)} %bitcast.60), kind=kOutput, calls=%fused_computation.11 | convolution fusion | flops 2150105088 | bytes 10485760 | tf_op jit(solution)/shard_map/dot_general | solution.py:178
  556.8 9.8 %reduce-scatter.2.cloned.1.call-done = bf16[256,1024]{1,0:T(8,128)(2,1)} async-done(((bf16[256,2048]{1,0:T(8,128)(2,1)}), bf16[256,1024]{1,0:T(8,128)(2,1)}) %reduce-scatter.2.cloned.1.call-update) | async-done | bytes 524304 | tf_op jit(solution)/shard_map/reduce_scatter | solution.py:183
  (80 shorter events, 21.6 us)
Async XLA Ops:
  6.5 337.4 %copy-start = (bf16[4,256,256]{2,1,0:T(8,128)(2,1)S(1)}, bf16[4,256,256]{2,1,0:T(8,128)(2,1)}, u32[]{:S(2)}) copy-start(bf16[4,256,256]{2,1,0:T(8,128)(2,1)} %param.18) | copy-start | bytes 1572868
  6.5 80.3 %copy-start.3 = (bf16[1,256,2048]{2,1,0:T(8,128)(2,1)S(1)}, bf16[1,256,2048]{2,1,0:T(8,128)(2,1)}, u32[]{:S(2)}) copy-start(bf16[1,256,2048]{2,1,0:T(8,128)(2,1)} %param.12) | copy-start | bytes 3145732
  6.5 80.3 %copy-start.10 = (f32[2048]{0:T(1024)S(1)}, f32[2048]{0:T(1024)}, u32[]{:S(2)}) copy-start(f32[2048]{0:T(1024)} %param.13) | copy-start | bytes 24580
  6.5 80.3 %all-gather.10.cloned.1.call-start = ((), (), s32[]{:S(2)}) async-start(), calls=%async_computation.2 | async-start | bytes 4456448 | tf_op jit(solution)/shard_map/all_gather | solution.py:59
  7.3 156.6 %all-gather.12.cloned.1.call-start = ((), (), s32[]{:S(2)}) async-start(), calls=%async_computation.3 | async-start | bytes 4456448 | tf_op jit(solution)/shard_map/all_gather | solution.py:60
  8.0 232.8 %all-gather.16.cloned.1.call-start = ((), (), s32[]{:S(2)}) async-start(), calls=%async_computation.5 | async-start | bytes 4456448 | tf_op jit(solution)/shard_map/all_gather | solution.py:61
  8.7 308.9 %all-gather.8.cloned.1.call-start = ((), (), s32[]{:S(2)}) async-start(), calls=%async_computation.1 | async-start | bytes 4456448 | tf_op jit(solution)/shard_map/all_gather | solution.py:58
  9.3 351.9 %all-gather.14.cloned.1.call-start = ((), (), s32[]{:S(2)}) async-start(), calls=%async_computation.4 | async-start | bytes 2621440 | tf_op jit(solution)/shard_map/all_gather | solution.py:110
  174.9 65.9 %copy-start.4 = (bf16[1,256,2048]{2,1,0:T(8,128)(2,1)S(1)}, bf16[1,256,2048]{2,1,0:T(8,128)(2,1)}, u32[]{:S(2)}) copy-start(bf16[1,256,2048]{2,1,0:T(8,128)(2,1)} %param.12) | copy-start | bytes 3145732
  176.3 68.9 %copy-start.6 = (bf16[1024,128]{1,0:T(8,128)(2,1)S(1)}, bf16[1024,128]{1,0:T(8,128)(2,1)}, u32[]{:S(2)}) copy-start(bf16[1024,128]{1,0:T(8,128)(2,1)} %param.23) | copy-start | bytes 786436
  176.3 68.9 %copy-start.7 = (bf16[1024,128]{1,0:T(8,128)(2,1)S(1)}, bf16[1024,128]{1,0:T(8,128)(2,1)}, u32[]{:S(2)}) copy-start(bf16[1024,128]{1,0:T(8,128)(2,1)} %param.22) | copy-start | bytes 786436
  176.3 231.7 %all-gather.18.cloned.1.call-start = ((), (), s32[]{:S(2)}) async-start(), calls=%async_computation.6 | async-start | bytes 2621440 | tf_op jit(solution)/shard_map/all_gather | solution.py:111
  245.1 72.5 %copy-start.5 = (bf16[1,256,2048]{2,1,0:T(8,128)(2,1)S(1)}, bf16[1,256,2048]{2,1,0:T(8,128)(2,1)}, u32[]{:S(2)}) copy-start(bf16[1,256,2048]{2,1,0:T(8,128)(2,1)} %param.12) | copy-start | bytes 3145732
  245.2 304.7 %all-gather.20.cloned.1.call-start = ((), (), s32[]{:S(2)}) async-start(), calls=%async_computation.7 | async-start | bytes 8912896 | tf_op jit(solution)/shard_map/all_gather | solution.py:180
  246.1 320.4 %reduce-scatter.2.cloned.1.call-start = ((), (), s32[]{:S(2)}) async-start(), calls=%async_computation.8 | async-start | bytes 1572864 | tf_op jit(solution)/shard_map/reduce_scatter | solution.py:183
  246.5 78.0 %copy-start.8 = (f32[1024]{0:T(1024)S(1)}, f32[1024]{0:T(1024)}, u32[]{:S(2)}) copy-start(f32[1024]{0:T(1024)} %param.19) | copy-start | bytes 12292
  246.5 78.0 %copy-start.11 = (f32[8]{0:T(128)S(1)}, f32[8]{0:T(128)}, u32[]{:S(2)}) copy-start(f32[8]{0:T(128)} %param.21) | copy-start | bytes 100
  321.2 5.8 %collective-permute-start = (bf16[15,1024]{1,0:T(8,128)(2,1)S(1)}, bf16[15,1024]{1,0:T(8,128)(2,1)S(1)}, u32[]{:S(2)}, u32[]{:S(2)}) collective-permute-start(bf16[15,1024]{1,0:T(8,128)(2,1)S(1)} %slice.77), channel_id=1, source_target_pairs={{0,8},{8,16},{16,24},{1,9},{9,17},{17,25},{2,10},{10,18},{18,26},{... | collective-permute-start | bytes 92168 | tf_op jit(solution)/shard_map/ppermute | solution.py:21
  343.5 17.8 %copy-start.2 = (bf16[256,4,2,64]{3,0,1,2:T(8,128)(2,1)S(1)}, bf16[256,4,2,64]{3,0,1,2:T(8,128)(2,1)}, u32[]{:S(2)}) copy-start(bf16[256,4,2,64]{3,0,1,2:T(8,128)(2,1)} %get-tuple-element.26) | copy-start | bytes 786436
  414.3 0.7 copy-start.9
  414.4 135.5 %copy-start.12 = (bf16[4,256,256]{1,2,0:T(8,128)(2,1)S(1)}, bf16[4,256,256]{1,2,0:T(8,128)(2,1)}, u32[]{:S(2)}) copy-start(bf16[4,256,256]{1,2,0:T(8,128)(2,1)} %fusion.13) | copy-start | bytes 1572868
  549.9 16.6 %copy-start.1 = (bf16[4,256,256]{2,1,0:T(8,128)(2,1)S(1)}, bf16[4,256,256]{2,1,0:T(8,128)(2,1)}, u32[]{:S(2)}) copy-start(bf16[4,256,256]{2,1,0:T(8,128)(2,1)} %param.18) | copy-start | bytes 1572868
Sparse Core Ops, SparseCore 0:
  10.1 76.6 all-gather.9
  89.6 74.1 all-gather.11
  166.6 74.1 all-gather.15
  243.5 74.1 all-gather.7
  319.1 42.1 all-gather.13
  362.7 45.2 all-gather.17
  410.7 139.1 all-gather.19
  556.9 9.5 reduce-scatter.1
where the time goes:
time: 575 us; the launch traced here: 573 us
  waiting for transfers between devices  486 us (85%)
  matrix products  31.7 us (6%)
  local copies, waits for them, and re-layouts  23 us (4%)
  other arithmetic  15.2 us (3%)
  between operations  13.8 us (2%)
    all_gather x1, waiting for transfers between devices, local(): lax.all_gather(out_local, ('sp', 'fs'), axis=1, tiled=True)  135 us
    all_gather x1, waiting for transfers between devices, local(): lax.all_gather(query_weight, ('sp', 'fs'), axis=0, tiled=True)  75.4 us
    all_gather x1, waiting for transfers between devices, local(): lax.all_gather(pool_input, ('sp', 'fs'), axis=0, tiled=True)  71.2 us
    all_gather x1, waiting for transfers between devices, local(): lax.all_gather(key_weight, ('sp', 'fs'), axis=0, tiled=True)  70.4 us
    all_gather x1, waiting for transfers between devices, local(): lax.all_gather(value_weight, ('sp', 'fs'), axis=0, tiled=True)  64.5 us
    all_gather x1, waiting for transfers between devices, local(): lax.all_gather(values_flat, 'sp', axis=0, tiled=True)  39.5 us
    dot_general x4, matrix products, local(): jnp.dot(normed, fragment, preferred_element_type=jnp.float32)  16.7 us
    all_gather x1, waiting for transfers between devices, local(): lax.all_gather(keys_flat, 'sp', axis=0, tiled=True)  16.2 us
  transfers between devices with their start and end apart: 9, of which 9 were waited for; matrix products, arithmetic and copies ran while one was open for 11% of the time, Pallas kernels for 0%

commit v1 on v0

--- a/solution.py
+++ b/solution.py
@@ -3,6 +3,8 @@
 import jax
 import jax.numpy as jnp
 from jax import lax
+from jax.experimental import pallas as pl
+from jax.experimental.pallas import tpu as pltpu
 from jax.sharding import PartitionSpec as P
 
 HEAD_DIM = 128
@@ -186,6 +188,561 @@
     return layer_out[None]
 
 
+MESH = pl.DeviceIdType.MESH
+
+def fused_kernel(
+    places,
+    groups,
+    normed_ref,
+    pool_ref,
+    query_ref,
+    key_ref,
+    value_ref,
+    map_ref,
+    scale_ref,
+    gain_ref,
+    lambda_ref,
+    out_pool_ref,
+    out_heads_ref,
+    cos_ref,
+    sin_ref,
+    out_ref,
+    rows_all,
+    weights,
+    outs,
+    queries,
+    keys,
+    values,
+    pools,
+    to_mate,
+    from_mate,
+    to_peer,
+    from_peer,
+    *sems,
+):
+    (
+        own_sem,
+        in_local,
+        in_z_send,
+        in_z_recv,
+        in_n_send,
+        in_n_recv,
+        in_f_send,
+        in_f_recv,
+        out_local,
+        out_z_send,
+        out_z_recv,
+        out_n_send,
+        out_n_recv,
+        out_f_send,
+        out_f_recv,
+        right_send,
+        right_recv,
+        left_send,
+        left_recv,
+        mate_send,
+        mate_recv,
+        half_send,
+        half_recv,
+        peer_send,
+        peer_recv,
+    ) = sems
+    z = lax.axis_index("sp")
+    f = lax.axis_index("fs")
+    c = lax.axis_index("tp")
+    fx = f + 1 - 2 * lax.rem(f, 2)
+    fy = lax.rem(f + 2, groups)
+    mate = 1 - c
+    half_rows = normed_ref.shape[0]
+    row_count = 2 * half_rows
+    depth = pool_ref.shape[0]
+    width = GROUP_DIM
+    out_width = out_pool_ref.shape[1]
+    half_out = out_ref.shape[1]
+
+    barrier = pltpu.get_barrier_semaphore()
+    partners = [{"sp": lax.rem(z + d, places)} for d in range(1, places)]
+    partners += [{"fs": fx}, {"fs": fy}, {"tp": mate}]
+    for partner in partners:
+        pl.semaphore_signal(barrier, inc=1, device_id=partner, device_id_type=MESH)
+    pl.semaphore_wait(barrier, len(partners))
+
+    def remote(source, target, send, recv, device):
+        return pltpu.make_async_remote_copy(
+            src_ref=source,
+            dst_ref=target,
+            send_sem=send,
+            recv_sem=recv,
+            device_id=device,
+            device_id_type=MESH,
+        )
+
+    def block(index, size):
+        return pl.ds(pl.multiple_of(index * size, size), size)
+
+    class Gather:
+        def __init__(self, sources, cut, view, group):
+            self.sources, self.cut, self.view = sources, cut, view
+            self.count = len(sources)
+            (
+                self.local,
+                self.z_send,
+                self.z_recv,
+                self.n_send,
+                self.n_recv,
+                self.f_send,
+                self.f_recv,
+            ) = group
+            self.low = (0, self.count // 2)
+            self.high = (self.count // 2, self.count - self.count // 2)
+
+        def own(self, m):
+            return pltpu.make_async_copy(
+                self.cut(self.sources[m], z), self.view(z, f, m, 1).at[0], self.local.at[m]
+            )
+
+        def across(self, d, m):
+            to = lax.rem(z + d, places)
+            return remote(
+                self.cut(self.sources[m], to),
+                self.view(z, f, m, 1).at[0],
+                self.z_send.at[d, m],
+                self.z_recv.at[d, m],
+                {"sp": to},
+            )
+
+        def arrive(self, d, m):
+            view = self.view(lax.rem(z + places - d, places), f, m, 1).at[0]
+            return remote(
+                view,
+                view,
+                self.z_send.at[d, m],
+                self.z_recv.at[d, m],
+                {"sp": lax.rem(z + places - d, places)},
+            )
+
+        def near(self, d, side, column):
+            view = self.view(lax.rem(z + places - d, places), column, 0, self.count)
+            return remote(
+                view,
+                view,
+                self.n_send.at[side, d],
+                self.n_recv.at[side, d],
+                {"fs": (fx, fy)[side]},
+            )
+
+        def forward(self, d, side, column):
+            start, size = (self.high, self.low)[side]
+            view = self.view(lax.rem(z + places - d, places), column, start, size)
+            return remote(
+                view,
+                view,
+                self.f_send.at[side, d],
+                self.f_recv.at[side, d],
+                {"fs": (fx, fy)[side]},
+            )
+
+        def start(self):
+            for m in range(self.count):
+                self.own(m).start()
+            for d in range(1, places):
+                for m in range(self.count):
+                    self.across(d, m).start()
+
+        def first(self, d):
+            for m in range(self.count):
+                if d == 0:
+                    self.own(m).wait()
+                else:
+                    self.arrive(d, m).wait_recv()
+            for side in range(2):
+                self.near(d, side, f).start()
+
+        def second(self, d):
+            self.near(d, 0, fx).wait_recv()
+            self.forward(d, 1, fx).start()
+            self.near(d, 1, fy).wait_recv()
+            self.forward(d, 0, fy).start()
+
+        def third(self, d):
+            diagonal = lax.rem(fx + 2, groups)
+            for side in range(2):
+                self.forward(d, side, diagonal).wait_recv()
+
+        def drain(self):
+            for d in range(places):
+                for m in range(self.count):
+                    if d > 0:
+                        self.across(d, m).wait_send()
+                for side in range(2):
+                    self.near(d, side, f).wait_send()
+                self.forward(d, 1, fx).wait_send()
+                self.forward(d, 0, fy).wait_send()
+
+    inward = Gather(
+        (pool_ref, query_ref, key_ref, value_ref),
+        lambda ref, to: ref.at[:, block(to, width)],
+        lambda zz, ff, m, n: weights.at[pl.ds(m, n), block(zz * groups + ff, depth), :],
+        (in_local, in_z_send, in_z_recv, in_n_send, in_n_recv, in_f_send, in_f_recv),
+    )
+    outward = Gather(
+        (out_pool_ref, out_heads_ref),
+        lambda ref, to: ref.at[block(to, width), :],
+        lambda zz, ff, m, n: outs.at[pl.ds(m, n), :, block(zz * groups + ff, out_width)],
+        (out_local, out_z_send, out_z_recv, out_n_send, out_n_recv, out_f_send, out_f_recv),
+    )
+
+    def chunk(zz, side):
+        return rows_all.at[block(2 * zz + side, half_rows), :]
+
+    def right(k):
+        view = chunk(z - k, c)
+        return remote(view, view, right_send.at[k], right_recv.at[k + 1], {"sp": z + 1})
+
+    def from_left(k):
+        view = chunk(z - k, c)
+        return remote(view, view, right_send.at[k], right_recv.at[k], {"sp": z - 1})
+
+    def left(k):
+        view = chunk(z + k, c)
+        return remote(view, view, left_send.at[k], left_recv.at[k + 1], {"sp": z - 1})
+
+    def from_right(k):
+        view = chunk(z + k, c)
+        return remote(view, view, left_send.at[k], left_recv.at[k], {"sp": z + 1})
+
+    def share(slot, zz, side):
+        view = chunk(zz, side)
+        return remote(view, view, mate_send.at[slot], mate_recv.at[slot], {"tp": mate})
+
+    own_rows = pltpu.make_async_copy(normed_ref, chunk(z, c), own_sem)
+    own_rows.start()
+    inward.start()
+    own_rows.wait()
+
+    @pl.when(z < places - 1)
+    def _():
+        right(0).start()
+
+    @pl.when(z > 0)
+    def _():
+        left(0).start()
+
+    share(0, z, c).start()
+
+    def tokens_step(k):
+        @pl.when(z >= k)
+        def _():
+            from_left(k).wait_recv()
+
+            @pl.when(z < places - 1)
+            def _():
+                right(k).start()
+
+            share(k, z - k, c).start()
+
+        @pl.when(z + k < places)
+        def _():
+            from_right(k).wait_recv()
+
+            @pl.when(z > 0)
+            def _():
+                left(k).start()
+
+            share(places - 1 + k, z + k, c).start()
+
+    for d in range(places):
+        inward.first(d)
+        if d > 0:
+            inward.second(d - 1)
+    pools[0:16, :] = jnp.zeros((16, width), jnp.bfloat16)
+    tokens_step(1)
+    inward.second(places - 1)
+    for k in range(2, places):
+        tokens_step(k)
+    outward.start()
+    for d in range(places):
+        inward.third(d)
+
+    share(0, z, mate).wait_recv()
+    for k in range(1, places):
+
+        @pl.when(z >= k)
+        def _():
+            share(k, z - k, mate).wait_recv()
+
+        @pl.when(z + k < places)
+        def _():
+            share(places - 1 + k, z + k, mate).wait_recv()
+
+    def turned(raw, cosine, sine):
+        floated = raw.astype(jnp.float32)
+        return (floated * cosine + pltpu.roll(floated, HEAD_DIM // 2, 1) * sine).astype(
+            jnp.bfloat16
+        )
+
+    def project(index, carry):
+        rows = block(index, row_count)
+        normed = rows_all[rows, :]
+        cosine = cos_ref[rows, :]
+        sine = sin_ref[rows, :]
+
+        def product(m):
+            return jnp.dot(normed, weights[m], preferred_element_type=jnp.float32).astype(
+                jnp.bfloat16
+            )
+
+        pools[pl.ds(pl.multiple_of(index * row_count + 16, 16), row_count), :] = product(0)
+        raw = product(1)
+        for m in range(2):
+            part = slice(m * HEAD_DIM, (m + 1) * HEAD_DIM)
+            queries[rows, part] = turned(raw[:, part], cosine, sine)
+        raw = product(2)
+        for m in range(2):
+            part = slice(m * HEAD_DIM, (m + 1) * HEAD_DIM)
+            keys[rows, part] = turned(raw[:, part], cosine, sine)
+        values[rows, :] = product(3)
+        return carry
+
+    outward.first(0)
+    lax.fori_loop(0, places, project, 0)
+    for d in range(1, places):
+        outward.first(d)
+        outward.second(d - 1)
+    outward.second(places - 1)
+    for d in range(places):
+        outward.third(d)
+
+    level = lax.rem(c * map_ref.shape[0] + z, 4)
+    window = jnp.where(
+        level == 0, 2, jnp.where(level == 1, 4, jnp.where(level == 2, 8, 16))
+    )
+    head_lambda = lambda_ref[c * map_ref.shape[0] + z]
+    length = places * row_count
+
+    def to_sibling(d, to):
+        return remote(
+            to_mate.at[to], from_mate.at[to], half_send.at[d], half_recv.at[d], {"tp": mate}
+        )
+
+    def to_place(d, to):
+        return remote(
+            to_peer.at[to], from_peer.at[d], peer_send.at[d], peer_recv.at[d], {"sp": to}
+        )
+
+    def compute(step, carry):
+        d = lax.rem(step + 1, places)
+        to = lax.rem(z + d, places)
+        rows = block(to, row_count)
+        query_pos = to * row_count + lax.broadcasted_iota(jnp.int32, (row_count, length), 0)
+        key_pos = lax.broadcasted_iota(jnp.int32, (row_count, length), 1)
+        seen = query_pos >= key_pos
+        mapped = []
+        for m in range(2):
+            part = slice(m * HEAD_DIM, (m + 1) * HEAD_DIM)
+            scores = lax.dot_general(
+                queries[rows, part],
+                keys[:, part],
+                (((1,), (1,)), ((), ())),
+                preferred_element_type=jnp.float32,
+            ) * HEAD_DIM ** (-0.5)
+            scores = jnp.where(seen, scores, -jnp.inf)
+            expons = jnp.exp(scores - jnp.max(scores, -1, keepdims=True))
+            totals = jnp.sum(expons, -1, keepdims=True)
+            mapped.append(
+                jnp.dot(
+                    expons.astype(jnp.bfloat16), values[...], preferred_element_type=jnp.float32
+                )
+                / totals
+            )
+        raw = mapped[0] - head_lambda * mapped[1]
+        attn = (
+            raw
+            * lax.rsqrt(jnp.mean(raw * raw, -1, keepdims=True) + HEAD_EPS)
+            * gain_ref[...]
+            * HEAD_SCALE
+        ).astype(jnp.bfloat16)
+        extended = pools[
+            pl.ds(pl.multiple_of(to * row_count, 16), row_count + 16), :
+        ].astype(jnp.float32)
+        picked = extended + pltpu.roll(extended, 1, 0)
+        sums = picked
+        for shift in (2, 4, 8):
+            sums = sums + pltpu.roll(sums, shift, 0)
+            picked = lax.select_n(window >= 2 * shift, picked, sums)
+        places_of = to * row_count + lax.broadcasted_iota(jnp.int32, (row_count, 1), 0)
+        counts = jnp.minimum(places_of + 1, window).astype(jnp.float32)
+        mixed = (picked[16:] / counts - extended[16:]).astype(jnp.bfloat16)
+        pooled = (
+            jnp.dot(mixed, map_ref[z], preferred_element_type=jnp.float32) * scale_ref[z]
+        ).astype(jnp.bfloat16)
+
+        def partial_of(side):
+            columns = block(side, half_out)
+            return jnp.dot(
+                pooled, outs[0, :, columns], preferred_element_type=jnp.float32
+            ) + jnp.dot(attn, outs[1, :, columns], preferred_element_type=jnp.float32)
+
+        to_mate[to] = partial_of(mate).astype(jnp.bfloat16)
+        to_sibling(d, to).start()
+        mine = partial_of(c)
+        to_sibling(d, to).wait_recv()
+        summed = mine + from_mate[to].astype(jnp.float32)
+
+        to_peer[to] = summed.astype(jnp.bfloat16)
+
+        @pl.when(d > 0)
+        def _():
+            to_place(d, to).start()
+
+        return carry
+
+    lax.fori_loop(0, places, compute, 0)
+
+    total = to_peer[z].astype(jnp.float32)
+    for d in range(1, places):
+        to_place(d, lax.rem(z + d, places)).wait_recv()
+        total = total + from_peer[d].astype(jnp.float32)
+    out_ref[...] = total.astype(out_ref.dtype)
+
+    inward.drain()
+    outward.drain()
+
+    @pl.when(z < places - 1)
+    def _():
+        right(0).wait_send()
+
+    @pl.when(z > 0)
+    def _():
+        left(0).wait_send()
+
+    share(0, z, c).wait_send()
+    for k in range(1, places):
+
+        @pl.when(z >= k)
+        def _():
+            @pl.when(z < places - 1)
+            def _():
+                right(k).wait_send()
+
+            share(k, z - k, c).wait_send()
+
+        @pl.when(z + k < places)
+        def _():
+            @pl.when(z > 0)
+            def _():
+                left(k).wait_send()
+
+            share(places - 1 + k, z + k, c).wait_send()
+
+    for d in range(places):
+        to = lax.rem(z + d, places)
+        to_sibling(d, to).wait_send()
+        if d > 0:
+            to_place(d, to).wait_send()
+
+
+def fused(
+    tokens,
+    norm_gain,
+    pool_input,
+    query_weight,
+    key_weight,
+    value_weight,
+    pool_map,
+    pool_scale,
+    head_gain,
+    diff_lambda,
+    out_pool,
+    out_heads,
+):
+    places = lax.axis_size("sp")
+    groups = lax.axis_size("fs")
+    row_count, model = tokens.shape[1], tokens.shape[2]
+    half_rows = row_count // 2
+    floated = lax.dynamic_slice_in_dim(
+        tokens[0], lax.axis_index("tp") * half_rows, half_rows, 0
+    ).astype(jnp.float32)
+    normed = (
+        floated * lax.rsqrt(jnp.mean(floated * floated, -1, keepdims=True) + NORM_EPS) * norm_gain
+    ).astype(jnp.bfloat16)
+    length = places * row_count
+    half = HEAD_DIM // 2
+    freqs = 1.0 / THETA ** (jnp.arange(half, dtype=jnp.float32) * 2.0 / HEAD_DIM)
+    angles = jnp.arange(length, dtype=jnp.float32)[:, None] * freqs[None, :]
+    cosine, sine = jnp.cos(angles), jnp.sin(angles)
+    cosine = jnp.concatenate([cosine, cosine], 1)
+    sine = jnp.concatenate([-sine, sine], 1)
+    group_count = pool_map.shape[0]
+    half_out = model // 2
+    vmem = pl.BlockSpec(memory_space=pltpu.VMEM)
+    smem = pl.BlockSpec(memory_space=pltpu.SMEM)
+    dma = pltpu.SemaphoreType.DMA
+    low = jnp.bfloat16
+
+    def gather_sems(count):
+        return [
+            dma((count,)),
+            dma((places, count)),
+            dma((places, count)),
+            dma((2, places)),
+            dma((2, places)),
+            dma((2, places)),
+            dma((2, places)),
+        ]
+
+    out = pl.pallas_call(
+        lambda *refs: fused_kernel(places, groups, *refs),
+        out_shape=jax.ShapeDtypeStruct((row_count, half_out), low),
+        in_specs=[vmem] * 8 + [smem] + [vmem] * 4,
+        out_specs=vmem,
+        scratch_shapes=[
+            pltpu.VMEM((length, model), low),
+            pltpu.VMEM((4, model, GROUP_DIM), low),
+            pltpu.VMEM((2, GROUP_DIM, model), low),
+            pltpu.VMEM((length, GROUP_DIM), low),
+            pltpu.VMEM((length, GROUP_DIM), low),
+            pltpu.VMEM((length, GROUP_DIM), low),
+            pltpu.VMEM((length + 16, GROUP_DIM), low),
+            pltpu.VMEM((places, row_count, half_out), low),
+            pltpu.VMEM((places, row_count, half_out), low),
+            pltpu.VMEM((places, row_count, half_out), low),
+            pltpu.VMEM((places, row_count, half_out), low),
+            dma,
+            *gather_sems(4),
+            *gather_sems(2),
+            dma((places,)),
+            dma((places + 1,)),
+            dma((places,)),
+            dma((places + 1,)),
+            dma((2 * places,)),
+            dma((2 * places,)),
+            dma((places,)),
+            dma((places,)),
+            dma((places,)),
+            dma((places,)),
+        ],
+        compiler_params=pltpu.CompilerParams(
+            collective_id=0, has_side_effects=True, vmem_limit_bytes=56 * 1024 * 1024
+        ),
+    )(
+        normed,
+        pool_input,
+        query_weight,
+        key_weight,
+        value_weight,
+        pool_map,
+        pool_scale.reshape(group_count, 1, GROUP_DIM),
+        head_gain.reshape(1, 2 * HEAD_DIM),
+        diff_lambda,
+        out_pool,
+        out_heads,
+        cosine,
+        sine,
+    )
+    return out[None]
+
+
 def solution(mesh):
     placed = (
         P("fs", "sp", None),
@@ -201,6 +758,19 @@
         P("tp", ("sp", "fs")),
         P("tp", ("sp", "fs")),
     )
+    shape = dict(mesh.shape)
+
+    def body(tokens, *rest):
+        head_count = rest[3].shape[1] // (2 * HEAD_DIM)
+        group_count = rest[5].shape[0]
+        fits = (
+            shape["fs"] == 4
+            and shape["tp"] == 2
+            and shape["sp"] == head_count == group_count
+            and tokens.shape[0] == 1
+        )
+        return (fused if fits else local)(tokens, *rest)
+
     return jax.shard_map(
-        local, mesh=mesh, in_specs=placed, out_specs=P("fs", "sp", "tp"), check_vma=False
-    )
+        body, mesh=mesh, in_specs=placed, out_specs=P("fs", "sp", "tp"), check_vma=False
+    )

time: 575 us -> 150 us (0.26)
  waiting for transfers between devices: 486 us -> 0 us
  Pallas kernels: 0 us -> 141 us
  matrix products: 31.7 us -> 0 us
  local copies, waits for them, and re-layouts: 23 us -> 1.87 us
  between operations: 13.8 us -> 0.02 us
  other arithmetic: 15.2 us -> 6.58 us
    all_gather x7 -> x0, waiting for transfers between devices: 472 us -> none  [the longest x1 135 us: local(): lax.all_gather(out_local, ('sp', 'fs'), axis=1, tiled=True)]
    pallas_call x0 -> x1, Pallas kernels: none -> 141 us  [fused(): pl.pallas_call(lambda *refs: fused_kernel(places, groups, *refs), out_sha...]
    dot_general x8 -> x0, matrix products: 31.7 us -> none  [the longest x4 16.7 us: local(): jnp.dot(normed, fragment, preferred_element_type=jnp.float32)]
    reduce_scatter x1 -> x0, waiting for transfers between devices: 9.76 us -> none  [local(): lax.psum_scatter(partial_value.astype(jnp.bfloat16), 'tp', scatter_dimens...]
    another operation x4 -> x0, local copies, waits for them, and re-layouts: 9.58 us -> none  [local(): jnp.stack([pair_sums[14:14 + row_count], quad_sums[12:12 + row_count], oc...]
  transfers between devices with their start and end apart: 9 -> 0, of which waited for: 9 -> 0; matrix products, arithmetic and copies ran while one was open for 11% -> 0% of each run, Pallas kernels for 0% -> 0%
where the time goes in v1:
time: 150 us; the launch traced here: 149 us
  Pallas kernels  141 us (94%)
  other arithmetic  6.58 us (4%)
  local copies, waits for them, and re-layouts  1.87 us (1%)
    pallas_call x1, Pallas kernels, fused(): pl.pallas_call(lambda *refs: fused_kernel(places, groups, *refs), out_sha...  141 us

profile of v1, /device:TPU:10, one launch (start us, length us, event | category | flops | bytes accessed | tf_op | source)
XLA Modules:
  0.0 149.1 jit_solution(3108069761628711427)
XLA Ops:
  0.0 0.0 copy-start
  0.0 1.2 fusion
  1.3 0.0 copy-done
  1.3 2.0 %fusion.2.refs_0_ = bf16[128,2048]{1,0:T(8,128)(2,1)} fusion(f32[2048]{0:T(1024)S(1)} %copy-done, f32[128]{0:T(128)S(1)} %add_rsqrt_fusion, bf16[1,256,2048]{2,1,0:T(8,128)(2,1)} %param.12, s32[]{:T(128)S(6)} %select_n.3), kind=kLoop, calls=%fused_computation.4 | loop fusion | flops 1048576 | bytes 1057284 | tf_op jit(solution)/shard_map/convert_element_type | solution.py:668
  3.3 2.0 %fusion.5 = (f32[1024,64]{1,0:T(8,128)S(1)}, f32[1024,64]{1,0:T(8,128)S(1)}, f32[1024,64]{1,0:T(8,128)S(1)}) fusion(f32[64]{0:T(128)S(1)} %negate_power_fusion), kind=kLoop, calls=%fused_computation.10 | loop fusion | flops 131072 | bytes 786688 | tf_op jit(solution)/shard_map/neg | solution.py:675
  5.3 1.3 pad_maximum_fusion
  6.6 140.6 %shard_map.118 = bf16[256,1024]{1,0:T(8,128)(2,1)} custom-call(bf16[128,2048]{1,0:T(8,128)(2,1)} %fusion.2.refs_0_, bf16[128,1024]{1,0:T(8,128)(2,1)} %refs_1_.1, bf16[128,1024]{1,0:T(8,128)(2,1)} %refs_2_.1, bf16[128,1024]{1,0:T(8,128)(2,1)} %refs_3_.1, bf16[128,1024]{1,0:T(8,128)(2,1)} %refs_4_.1, bf16[4,256,256]{2,1,0:T(8,128)(2,1)} %refs_5_.1, ...), custom_call_target="tpu_custom_call" | custom-call | tf_op jit(solution)/shard_map/pallas_call | solution.py:694
  147.2 1.9 %copy.14 = bf16[1,256,1024]{2,1,0:T(8,128)(2,1)} copy(bf16[1,256,1024]{2,1,0:T(8,128)(2,1)} %bitcast.7) | data formatting | bytes 1048576
  (2 shorter events, 0.0 us)
Async XLA Ops:
  0.0 1.3 copy-start

commit v2 on v1

--- a/solution.py
+++ b/solution.py
@@ -189,6 +189,7 @@
 
 
 MESH = pl.DeviceIdType.MESH
+PIECES = 2
 
 def fused_kernel(
     places,
@@ -218,6 +219,8 @@
     from_mate,
     to_peer,
     from_peer,
+    merging,
+    final,
     *sems,
 ):
     (
@@ -246,6 +249,8 @@
         half_recv,
         peer_send,
         peer_recv,
+        merge_send,
+        merge_recv,
     ) = sems
     z = lax.axis_index("sp")
     f = lax.axis_index("fs")
@@ -392,88 +397,105 @@
         (out_local, out_z_send, out_z_recv, out_n_send, out_n_recv, out_f_send, out_f_recv),
     )
 
-    def chunk(zz, side):
-        return rows_all.at[block(2 * zz + side, half_rows), :]
-
-    def right(k):
-        view = chunk(z - k, c)
-        return remote(view, view, right_send.at[k], right_recv.at[k + 1], {"sp": z + 1})
-
-    def from_left(k):
-        view = chunk(z - k, c)
-        return remote(view, view, right_send.at[k], right_recv.at[k], {"sp": z - 1})
-
-    def left(k):
-        view = chunk(z + k, c)
-        return remote(view, view, left_send.at[k], left_recv.at[k + 1], {"sp": z - 1})
-
-    def from_right(k):
-        view = chunk(z + k, c)
-        return remote(view, view, left_send.at[k], left_recv.at[k], {"sp": z + 1})
-
-    def share(slot, zz, side):
-        view = chunk(zz, side)
-        return remote(view, view, mate_send.at[slot], mate_recv.at[slot], {"tp": mate})
-
-    own_rows = pltpu.make_async_copy(normed_ref, chunk(z, c), own_sem)
+    piece_rows = half_rows // PIECES
+
+    def chunk(zz, side, p):
+        return rows_all.at[block((2 * zz + side) * PIECES + p, piece_rows), :]
+
+    def right(k, p):
+        view = chunk(z - k, c, p)
+        return remote(view, view, right_send.at[k, p], right_recv.at[k + 1, p], {"sp": z + 1})
+
+    def from_left(k, p):
+        view = chunk(z - k, c, p)
+        return remote(view, view, right_send.at[k, p], right_recv.at[k, p], {"sp": z - 1})
+
+    def left(k, p):
+        view = chunk(z + k, c, p)
+        return remote(view, view, left_send.at[k, p], left_recv.at[k + 1, p], {"sp": z - 1})
+
+    def from_right(k, p):
+        view = chunk(z + k, c, p)
+        return remote(view, view, left_send.at[k, p], left_recv.at[k, p], {"sp": z + 1})
+
+    def share(slot, zz, side, p):
+        view = chunk(zz, side, p)
+        return remote(view, view, mate_send.at[slot, p], mate_recv.at[slot, p], {"tp": mate})
+
+    own_rows = pltpu.make_async_copy(
+        normed_ref, rows_all.at[block(2 * z + c, half_rows), :], own_sem
+    )
     own_rows.start()
     inward.start()
+    outward.start()
     own_rows.wait()
 
     @pl.when(z < places - 1)
     def _():
-        right(0).start()
+        for p in range(PIECES):
+            right(0, p).start()
 
     @pl.when(z > 0)
     def _():
-        left(0).start()
-
-    share(0, z, c).start()
+        for p in range(PIECES):
+            left(0, p).start()
+
+    for p in range(PIECES):
+        share(0, z, c, p).start()
 
     def tokens_step(k):
-        @pl.when(z >= k)
-        def _():
-            from_left(k).wait_recv()
-
-            @pl.when(z < places - 1)
+        for p in range(PIECES):
+
+            @pl.when(z >= k)
             def _():
-                right(k).start()
-
-            share(k, z - k, c).start()
-
-        @pl.when(z + k < places)
-        def _():
-            from_right(k).wait_recv()
-
-            @pl.when(z > 0)
+                from_left(k, p).wait_recv()
+
+                @pl.when(z < places - 1)
+                def _():
+                    right(k, p).start()
+
+                share(k, z - k, c, p).start()
+
+            @pl.when(z + k < places)
             def _():
-                left(k).start()
-
-            share(places - 1 + k, z + k, c).start()
-
+                from_right(k, p).wait_recv()
+
+                @pl.when(z > 0)
+                def _():
+                    left(k, p).start()
+
+                share(places - 1 + k, z + k, c, p).start()
+
+    pools[0:16, :] = jnp.zeros((16, width), jnp.bfloat16)
     for d in range(places):
         inward.first(d)
         if d > 0:
             inward.second(d - 1)
-    pools[0:16, :] = jnp.zeros((16, width), jnp.bfloat16)
+    outward.first(0)
+    inward.second(places - 1)
+    for d in range(1, places):
+        outward.first(d)
+        if d > 1:
+            outward.second(d - 2)
     tokens_step(1)
-    inward.second(places - 1)
+    for d in (places - 2, places - 1):
+        outward.second(d)
     for k in range(2, places):
         tokens_step(k)
-    outward.start()
     for d in range(places):
         inward.third(d)
 
-    share(0, z, mate).wait_recv()
-    for k in range(1, places):
-
-        @pl.when(z >= k)
-        def _():
-            share(k, z - k, mate).wait_recv()
-
-        @pl.when(z + k < places)
-        def _():
-            share(places - 1 + k, z + k, mate).wait_recv()
+    for p in range(PIECES):
+        share(0, z, mate, p).wait_recv()
+        for k in range(1, places):
+
+            @pl.when(z >= k)
+            def _():
+                share(k, z - k, mate, p).wait_recv()
+
+            @pl.when(z + k < places)
+            def _():
+                share(places - 1 + k, z + k, mate, p).wait_recv()
 
     def turned(raw, cosine, sine):
         floated = raw.astype(jnp.float32)
@@ -504,12 +526,7 @@
         values[rows, :] = product(3)
         return carry
 
-    outward.first(0)
     lax.fori_loop(0, places, project, 0)
-    for d in range(1, places):
-        outward.first(d)
-        outward.second(d - 1)
-    outward.second(places - 1)
     for d in range(places):
         outward.third(d)
 
@@ -525,14 +542,30 @@
             to_mate.at[to], from_mate.at[to], half_send.at[d], half_recv.at[d], {"tp": mate}
         )
 
-    def to_place(d, to):
+    outer = (z == 0) | (z == places - 1)
+    pair = z + 1 - 2 * lax.rem(z, 2)
+    far = jnp.where(z < 2, places - 1, 0)
+    near = jnp.where(z < 2, 2, 1)
+
+    def to_inner(role, to):
         return remote(
-            to_peer.at[to], from_peer.at[d], peer_send.at[d], peer_recv.at[d], {"sp": to}
+            to_peer.at[to], merging.at[role], merge_send.at[role], merge_recv.at[role], {"sp": pair}
+        )
+
+    def to_place(role, to):
+        return remote(
+            to_peer.at[to], from_peer.at[0], peer_send.at[role], peer_recv.at[0], {"sp": to}
+        )
+
+    def to_pair():
+        return remote(
+            to_peer.at[pair], from_peer.at[1], peer_send.at[2], peer_recv.at[1], {"sp": pair}
         )
 
     def compute(step, carry):
-        d = lax.rem(step + 1, places)
-        to = lax.rem(z + d, places)
+        role = jnp.where((step == 3) | outer, step, lax.rem(step + 2, 3))
+        to = jnp.where(role == 0, far, jnp.where(role == 1, near, jnp.where(role == 2, pair, z)))
+        d = step
         rows = block(to, row_count)
         query_pos = to * row_count + lax.broadcasted_iota(jnp.int32, (row_count, length), 0)
         key_pos = lax.broadcasted_iota(jnp.int32, (row_count, length), 1)
@@ -589,57 +622,80 @@
         to_sibling(d, to).wait_recv()
         summed = mine + from_mate[to].astype(jnp.float32)
 
-        to_peer[to] = summed.astype(jnp.bfloat16)
-
-        @pl.when(d > 0)
+        @pl.when((role < 2) & outer)
         def _():
-            to_place(d, to).start()
+            to_peer[to] = summed.astype(jnp.bfloat16)
+            to_inner(role, to).start()
+
+        @pl.when((role < 2) & jnp.logical_not(outer))
+        def _():
+            to_inner(role, to).wait_recv()
+            to_peer[to] = (summed + merging[role].astype(jnp.float32)).astype(jnp.bfloat16)
+            to_place(role, to).start()
+
+        @pl.when(role == 2)
+        def _():
+            to_peer[to] = summed.astype(jnp.bfloat16)
+            to_pair().start()
+
+        @pl.when(role == 3)
+        def _():
+            final[...] = summed
 
         return carry
 
     lax.fori_loop(0, places, compute, 0)
 
-    total = to_peer[z].astype(jnp.float32)
-    for d in range(1, places):
-        to_place(d, lax.rem(z + d, places)).wait_recv()
-        total = total + from_peer[d].astype(jnp.float32)
-    out_ref[...] = total.astype(out_ref.dtype)
+    to_pair().wait_recv()
+    total = final[...] + from_peer[1].astype(jnp.float32)
+    to_place(0, z).wait_recv()
+    out_ref[...] = (total + from_peer[0].astype(jnp.float32)).astype(out_ref.dtype)
 
     inward.drain()
     outward.drain()
 
-    @pl.when(z < places - 1)
-    def _():
-        right(0).wait_send()
-
-    @pl.when(z > 0)
-    def _():
-        left(0).wait_send()
-
-    share(0, z, c).wait_send()
-    for k in range(1, places):
-
-        @pl.when(z >= k)
+    for p in range(PIECES):
+
+        @pl.when(z < places - 1)
         def _():
-            @pl.when(z < places - 1)
+            right(0, p).wait_send()
+
+        @pl.when(z > 0)
+        def _():
+            left(0, p).wait_send()
+
+        share(0, z, c, p).wait_send()
+        for k in range(1, places):
+
+            @pl.when(z >= k)
             def _():
-                right(k).wait_send()
-
-            share(k, z - k, c).wait_send()
-
-        @pl.when(z + k < places)
+                @pl.when(z < places - 1)
+                def _():
+                    right(k, p).wait_send()
+
+                share(k, z - k, c, p).wait_send()
+
+            @pl.when(z + k < places)
+            def _():
+                @pl.when(z > 0)
+                def _():
+                    left(k, p).wait_send()
+
+                share(places - 1 + k, z + k, c, p).wait_send()
+
+    for d in range(places):
+        to_sibling(d, d).wait_send()
+    for role, to in ((0, far), (1, near)):
+
+        @pl.when(outer)
         def _():
-            @pl.when(z > 0)
-            def _():
-                left(k).wait_send()
-
-            share(places - 1 + k, z + k, c).wait_send()
-
-    for d in range(places):
-        to = lax.rem(z + d, places)
-        to_sibling(d, to).wait_send()
-        if d > 0:
-            to_place(d, to).wait_send()
+            to_inner(role, to).wait_send()
+
+        @pl.when(jnp.logical_not(outer))
+        def _():
+            to_place(role, to).wait_send()
+
+    to_pair().wait_send()
 
 
 def fused(
@@ -707,20 +763,24 @@
             pltpu.VMEM((places, row_count, half_out), low),
             pltpu.VMEM((places, row_count, half_out), low),
             pltpu.VMEM((places, row_count, half_out), low),
-            pltpu.VMEM((places, row_count, half_out), low),
+            pltpu.VMEM((2, row_count, half_out), low),
+            pltpu.VMEM((2, row_count, half_out), low),
+            pltpu.VMEM((row_count, half_out), jnp.float32),
             dma,
             *gather_sems(4),
             *gather_sems(2),
-            dma((places,)),
-            dma((places + 1,)),
-            dma((places,)),
-            dma((places + 1,)),
-            dma((2 * places,)),
-            dma((2 * places,)),
+            dma((places, PIECES)),
+            dma((places + 1, PIECES)),
+            dma((places, PIECES)),
+            dma((places + 1, PIECES)),
+            dma((2 * places, PIECES)),
+            dma((2 * places, PIECES)),
             dma((places,)),
             dma((places,)),
-            dma((places,)),
-            dma((places,)),
+            dma((3,)),
+            dma((2,)),
+            dma((2,)),
+            dma((2,)),
         ],
         compiler_params=pltpu.CompilerParams(
             collective_id=0, has_side_effects=True, vmem_limit_bytes=56 * 1024 * 1024
@@ -766,7 +826,7 @@
         fits = (
             shape["fs"] == 4
             and shape["tp"] == 2
-            and shape["sp"] == head_count == group_count
+            and shape["sp"] == head_count == group_count == 4
             and tokens.shape[0] == 1
         )
         return (fused if fits else local)(tokens, *rest)

time: 150 us -> 133 us (0.89)
  Pallas kernels: 141 us -> 125 us
    pallas_call x1, Pallas kernels: 141 us -> 125 us  [fused(): pl.pallas_call(lambda *refs: fused_kernel(places, groups, *refs), out_sha...]
where the time goes in v2:
time: 133 us
  Pallas kernels  125 us (94%)
  other arithmetic  6.58 us (5%)
  local copies, waits for them, and re-layouts  1.87 us (1%)
    pallas_call x1, Pallas kernels, fused(): pl.pallas_call(lambda *refs: fused_kernel(places, groups, *refs), out_sha...  125 us

profile of v2, /device:TPU:10, one launch (start us, length us, event | category | flops | bytes accessed | tf_op | source)
XLA Modules:
  0.0 133.0 jit_solution(15788915514417658662)
XLA Ops:
  0.0 0.0 copy-start
  0.0 1.2 fusion
  1.3 0.0 copy-done
  1.3 2.0 %fusion.2.refs_0_ = bf16[128,2048]{1,0:T(8,128)(2,1)} fusion(f32[2048]{0:T(1024)S(1)} %copy-done, f32[128]{0:T(128)S(1)} %add_rsqrt_fusion, bf16[1,256,2048]{2,1,0:T(8,128)(2,1)} %param.12, s32[]{:T(128)S(6)} %select_n.3), kind=kLoop, calls=%fused_computation.4 | loop fusion | flops 1048576 | bytes 1057284 | tf_op jit(solution)/shard_map/convert_element_type | solution.py:724
  3.3 2.0 %fusion.5 = (f32[1024,64]{1,0:T(8,128)S(1)}, f32[1024,64]{1,0:T(8,128)S(1)}, f32[1024,64]{1,0:T(8,128)S(1)}) fusion(f32[64]{0:T(128)S(1)} %negate_power_fusion), kind=kLoop, calls=%fused_computation.10 | loop fusion | flops 131072 | bytes 786688 | tf_op jit(solution)/shard_map/neg | solution.py:731
  5.3 1.3 %pad_maximum_fusion = (f32[1024,128]{1,0:T(8,128)}, f32[1024,128]{1,0:T(8,128)}) fusion(f32[1024,64]{1,0:T(8,128)S(1)} %get-tuple-element.7, f32[1024,64]{1,0:T(8,128)S(1)} %get-tuple-element.6, f32[1024,64]{1,0:T(8,128)S(1)} %get-tuple-element.5), kind=kLoop, calls=%fused_computation.5 | loop fusion | flops 262144 | bytes 1835008 | tf_op jit(solution)/shard_map/concatenate | solution.py:730
  6.6 124.6 %shard_map.118 = bf16[256,1024]{1,0:T(8,128)(2,1)} custom-call(bf16[128,2048]{1,0:T(8,128)(2,1)} %fusion.2.refs_0_, bf16[128,1024]{1,0:T(8,128)(2,1)} %refs_1_.1, bf16[128,1024]{1,0:T(8,128)(2,1)} %refs_2_.1, bf16[128,1024]{1,0:T(8,128)(2,1)} %refs_3_.1, bf16[128,1024]{1,0:T(8,128)(2,1)} %refs_4_.1, bf16[4,256,256]{2,1,0:T(8,128)(2,1)} %refs_5_.1, ...), custom_call_target="tpu_custom_call" | custom-call | tf_op jit(solution)/shard_map/pallas_call | solution.py:750
  131.2 1.9 %copy.14 = bf16[1,256,1024]{2,1,0:T(8,128)(2,1)} copy(bf16[1,256,1024]{2,1,0:T(8,128)(2,1)} %bitcast.7) | data formatting | bytes 1048576
  (2 shorter events, 0.0 us)
Async XLA Ops:
  0.0 1.3 copy-start

commit v3 on v2

--- a/solution.py
+++ b/solution.py
@@ -194,7 +194,9 @@
 def fused_kernel(
     places,
     groups,
-    normed_ref,
+    tokens_ref,
+    norm_gain_ref,
+    freqs_ref,
     pool_ref,
     query_ref,
     key_ref,
@@ -205,9 +207,10 @@
     lambda_ref,
     out_pool_ref,
     out_heads_ref,
+    out_ref,
+    normed_ref,
     cos_ref,
     sin_ref,
-    out_ref,
     rows_all,
     weights,
     outs,
@@ -258,7 +261,7 @@
     fx = f + 1 - 2 * lax.rem(f, 2)
     fy = lax.rem(f + 2, groups)
     mate = 1 - c
-    half_rows = normed_ref.shape[0]
+    half_rows = tokens_ref.shape[0] // 2
     row_count = 2 * half_rows
     depth = pool_ref.shape[0]
     width = GROUP_DIM
@@ -425,9 +428,17 @@
     own_rows = pltpu.make_async_copy(
         normed_ref, rows_all.at[block(2 * z + c, half_rows), :], own_sem
     )
-    own_rows.start()
     inward.start()
     outward.start()
+    floated = tokens_ref[pl.ds(pl.multiple_of(c * half_rows, 16), half_rows), :].astype(
+        jnp.float32
+    )
+    normed_ref[...] = (
+        floated
+        * lax.rsqrt(jnp.mean(floated * floated, -1, keepdims=True) + NORM_EPS)
+        * norm_gain_ref[...]
+    ).astype(jnp.bfloat16)
+    own_rows.start()
     own_rows.wait()
 
     @pl.when(z < places - 1)
@@ -467,10 +478,25 @@
                 share(places - 1 + k, z + k, c, p).start()
 
     pools[0:16, :] = jnp.zeros((16, width), jnp.bfloat16)
-    for d in range(places):
+    inward.first(0)
+
+    def table(index, carry):
+        rows = block(index, row_count)
+        half = HEAD_DIM // 2
+        count = (
+            index * row_count + lax.broadcasted_iota(jnp.int32, (row_count, HEAD_DIM), 0)
+        ).astype(jnp.float32)
+        lane = lax.broadcasted_iota(jnp.int32, (row_count, HEAD_DIM), 1)
+        angles = count * freqs_ref[...]
+        cos_ref[rows, :] = jnp.cos(angles)
+        sine = jnp.sin(angles)
+        sin_ref[rows, :] = jnp.where(lane < half, -sine, sine)
+        return carry
+
+    lax.fori_loop(0, places, table, 0)
+    for d in range(1, places):
         inward.first(d)
-        if d > 0:
-            inward.second(d - 1)
+        inward.second(d - 1)
     outward.first(0)
     inward.second(places - 1)
     for d in range(1, places):
@@ -715,20 +741,10 @@
     places = lax.axis_size("sp")
     groups = lax.axis_size("fs")
     row_count, model = tokens.shape[1], tokens.shape[2]
-    half_rows = row_count // 2
-    floated = lax.dynamic_slice_in_dim(
-        tokens[0], lax.axis_index("tp") * half_rows, half_rows, 0
-    ).astype(jnp.float32)
-    normed = (
-        floated * lax.rsqrt(jnp.mean(floated * floated, -1, keepdims=True) + NORM_EPS) * norm_gain
-    ).astype(jnp.bfloat16)
     length = places * row_count
     half = HEAD_DIM // 2
     freqs = 1.0 / THETA ** (jnp.arange(half, dtype=jnp.float32) * 2.0 / HEAD_DIM)
-    angles = jnp.arange(length, dtype=jnp.float32)[:, None] * freqs[None, :]
-    cosine, sine = jnp.cos(angles), jnp.sin(angles)
-    cosine = jnp.concatenate([cosine, cosine], 1)
-    sine = jnp.concatenate([-sine, sine], 1)
+    freqs = jnp.concatenate([freqs, freqs])[None, :]
     group_count = pool_map.shape[0]
     half_out = model // 2
     vmem = pl.BlockSpec(memory_space=pltpu.VMEM)
@@ -750,9 +766,12 @@
     out = pl.pallas_call(
         lambda *refs: fused_kernel(places, groups, *refs),
         out_shape=jax.ShapeDtypeStruct((row_count, half_out), low),
-        in_specs=[vmem] * 8 + [smem] + [vmem] * 4,
+        in_specs=[vmem] * 10 + [smem] + [vmem] * 2,
         out_specs=vmem,
         scratch_shapes=[
+            pltpu.VMEM((row_count // 2, model), low),
+            pltpu.VMEM((length, HEAD_DIM), jnp.float32),
+            pltpu.VMEM((length, HEAD_DIM), jnp.float32),
             pltpu.VMEM((length, model), low),
             pltpu.VMEM((4, model, GROUP_DIM), low),
             pltpu.VMEM((2, GROUP_DIM, model), low),
@@ -786,7 +805,9 @@
             collective_id=0, has_side_effects=True, vmem_limit_bytes=56 * 1024 * 1024
         ),
     )(
-        normed,
+        tokens[0],
+        norm_gain.reshape(1, model),
+        freqs,
         pool_input,
         query_weight,
         key_weight,
@@ -797,8 +818,6 @@
         diff_lambda,
         out_pool,
         out_heads,
-        cosine,
-        sine,
     )
     return out[None]
 

time: 133 us -> 127 us (0.955)
  other arithmetic: 6.58 us -> 0.6 us
    convert_element_type x1 -> x0, other arithmetic: 2.03 us -> none  [fused(): normed = (floated * lax.rsqrt(jnp.mean(floated * floated, -1, keepdims=Tr...]
    neg x1 -> x0, other arithmetic: 1.96 us -> none  [fused(): sine = jnp.concatenate([-sine, sine], 1)]
    concatenate x1 -> x0, other arithmetic: 1.33 us -> none  [fused(): cosine = jnp.concatenate([cosine, cosine], 1)]
where the time goes in v3:
time: 127 us
  Pallas kernels  124 us (98%)
  local copies, waits for them, and re-layouts  1.87 us (1%)
    pallas_call x1, Pallas kernels, fused(): pl.pallas_call(lambda *refs: fused_kernel(places, groups, *refs), out_sha...  124 us

profile of v3, /device:TPU:10, one launch (start us, length us, event | category | flops | bytes accessed | tf_op | source)
XLA Modules:
  0.0 126.8 jit_solution(9494496066870630237)
XLA Ops:
  0.0 0.6 maximum_bitcast_fusion.refs_2_
  0.6 124.4 %shard_map.118 = bf16[256,1024]{1,0:T(8,128)(2,1)} custom-call(bf16[256,2048]{1,0:T(8,128)(2,1)} %bitcast.8, f32[1,2048]{1,0:T(1,128)} %bitcast.9, f32[1,128]{1,0:T(1,128)} %maximum_bitcast_fusion.refs_2_, bf16[128,1024]{1,0:T(8,128)(2,1)} %refs_3_.1, bf16[128,1024]{1,0:T(8,128)(2,1)} %refs_4_.1, bf16[128,1024]{1,0:T(8,128)(2,1)} %refs_5_.1, ...), custom_call_target="tpu_custom_call" | custom-call | tf_op jit(solution)/shard_map/pallas_call | solution.py:766
  125.0 1.9 %copy.14 = bf16[1,256,1024]{2,1,0:T(8,128)(2,1)} copy(bf16[1,256,1024]{2,1,0:T(8,128)(2,1)} %bitcast.7) | data formatting | bytes 1048576
  (1 shorter events, 0.0 us)

commit v4 on v3

--- a/solution.py
+++ b/solution.py
@@ -189,7 +189,8 @@
 
 
 MESH = pl.DeviceIdType.MESH
-PIECES = 2
+PIECES = 4
+PARTS = 2
 
 def fused_kernel(
     places,
@@ -329,13 +330,14 @@
                 {"sp": lax.rem(z + places - d, places)},
             )
 
-        def near(self, d, side, column):
-            view = self.view(lax.rem(z + places - d, places), column, 0, self.count)
+        def near(self, d, side, column, half):
+            start, size = (self.low, self.high)[half]
+            view = self.view(lax.rem(z + places - d, places), column, start, size)
             return remote(
                 view,
                 view,
-                self.n_send.at[side, d],
-                self.n_recv.at[side, d],
+                self.n_send.at[side, 2 * d + half],
+                self.n_recv.at[side, 2 * d + half],
                 {"fs": (fx, fy)[side]},
             )
 
@@ -363,19 +365,22 @@
                     self.own(m).wait()
                 else:
                     self.arrive(d, m).wait_recv()
-            for side in range(2):
-                self.near(d, side, f).start()
+            for order in range(2):
+                for side in range(2):
+                    self.near(d, side, f, side ^ order).start()
 
         def second(self, d):
-            self.near(d, 0, fx).wait_recv()
+            self.near(d, 0, fx, 0).wait_recv()
             self.forward(d, 1, fx).start()
-            self.near(d, 1, fy).wait_recv()
+            self.near(d, 1, fy, 1).wait_recv()
             self.forward(d, 0, fy).start()
 
         def third(self, d):
             diagonal = lax.rem(fx + 2, groups)
             for side in range(2):
                 self.forward(d, side, diagonal).wait_recv()
+            self.near(d, 0, fx, 1).wait_recv()
+            self.near(d, 1, fy, 0).wait_recv()
 
         def drain(self):
             for d in range(places):
@@ -383,7 +388,8 @@
                     if d > 0:
                         self.across(d, m).wait_send()
                 for side in range(2):
-                    self.near(d, side, f).wait_send()
+                    for half in range(2):
+                        self.near(d, side, f, half).wait_send()
                 self.forward(d, 1, fx).wait_send()
                 self.forward(d, 0, fy).wait_send()
 
@@ -563,9 +569,15 @@
     head_lambda = lambda_ref[c * map_ref.shape[0] + z]
     length = places * row_count
 
-    def to_sibling(d, to):
+    part_rows = row_count // PARTS
+
+    def to_sibling(step):
         return remote(
-            to_mate.at[to], from_mate.at[to], half_send.at[d], half_recv.at[d], {"tp": mate}
+            to_mate.at[step],
+            from_mate.at[step],
+            half_send.at[step],
+            half_recv.at[step],
+            {"tp": mate},
         )
 
     outer = (z == 0) | (z == places - 1)
@@ -573,28 +585,42 @@
     far = jnp.where(z < 2, places - 1, 0)
     near = jnp.where(z < 2, 2, 1)
 
-    def to_inner(role, to):
+    def to_inner(role, to, h):
         return remote(
-            to_peer.at[to], merging.at[role], merge_send.at[role], merge_recv.at[role], {"sp": pair}
-        )
-
-    def to_place(role, to):
+            to_peer.at[to * PARTS + h],
+            merging.at[role * PARTS + h],
+            merge_send.at[role * PARTS + h],
+            merge_recv.at[role * PARTS + h],
+            {"sp": pair},
+        )
+
+    def to_place(role, to, h):
         return remote(
-            to_peer.at[to], from_peer.at[0], peer_send.at[role], peer_recv.at[0], {"sp": to}
-        )
-
-    def to_pair():
+            to_peer.at[to * PARTS + h],
+            from_peer.at[h],
+            peer_send.at[role * PARTS + h],
+            peer_recv.at[h],
+            {"sp": to},
+        )
+
+    def to_pair(h):
         return remote(
-            to_peer.at[pair], from_peer.at[1], peer_send.at[2], peer_recv.at[1], {"sp": pair}
+            to_peer.at[pair * PARTS + h],
+            from_peer.at[PARTS + h],
+            peer_send.at[2 * PARTS + h],
+            peer_recv.at[PARTS + h],
+            {"sp": pair},
         )
 
     def compute(step, carry):
-        role = jnp.where((step == 3) | outer, step, lax.rem(step + 2, 3))
+        turn = step // PARTS
+        h = lax.rem(step, PARTS)
+        role = jnp.where((turn == 3) | outer, turn, lax.rem(turn + 2, 3))
         to = jnp.where(role == 0, far, jnp.where(role == 1, near, jnp.where(role == 2, pair, z)))
-        d = step
-        rows = block(to, row_count)
-        query_pos = to * row_count + lax.broadcasted_iota(jnp.int32, (row_count, length), 0)
-        key_pos = lax.broadcasted_iota(jnp.int32, (row_count, length), 1)
+        slot = to * PARTS + h
+        rows = block(slot, part_rows)
+        query_pos = slot * part_rows + lax.broadcasted_iota(jnp.int32, (part_rows, length), 0)
+        key_pos = lax.broadcasted_iota(jnp.int32, (part_rows, length), 1)
         seen = query_pos >= key_pos
         mapped = []
         for m in range(2):
@@ -622,14 +648,14 @@
             * HEAD_SCALE
         ).astype(jnp.bfloat16)
         extended = pools[
-            pl.ds(pl.multiple_of(to * row_count, 16), row_count + 16), :
+            pl.ds(pl.multiple_of(slot * part_rows, 16), part_rows + 16), :
         ].astype(jnp.float32)
         picked = extended + pltpu.roll(extended, 1, 0)
         sums = picked
         for shift in (2, 4, 8):
             sums = sums + pltpu.roll(sums, shift, 0)
             picked = lax.select_n(window >= 2 * shift, picked, sums)
-        places_of = to * row_count + lax.broadcasted_iota(jnp.int32, (row_count, 1), 0)
+        places_of = slot * part_rows + lax.broadcasted_iota(jnp.int32, (part_rows, 1), 0)
         counts = jnp.minimum(places_of + 1, window).astype(jnp.float32)
         mixed = (picked[16:] / counts - extended[16:]).astype(jnp.bfloat16)
         pooled = (
@@ -642,40 +668,45 @@
                 pooled, outs[0, :, columns], preferred_element_type=jnp.float32
             ) + jnp.dot(attn, outs[1, :, columns], preferred_element_type=jnp.float32)
 
-        to_mate[to] = partial_of(mate).astype(jnp.bfloat16)
-        to_sibling(d, to).start()
+        to_mate[step] = partial_of(mate).astype(jnp.bfloat16)
+        to_sibling(step).start()
         mine = partial_of(c)
-        to_sibling(d, to).wait_recv()
-        summed = mine + from_mate[to].astype(jnp.float32)
+        to_sibling(step).wait_recv()
+        summed = mine + from_mate[step].astype(jnp.float32)
 
         @pl.when((role < 2) & outer)
         def _():
-            to_peer[to] = summed.astype(jnp.bfloat16)
-            to_inner(role, to).start()
+            to_peer[slot] = summed.astype(jnp.bfloat16)
+            to_inner(role, to, h).start()
 
         @pl.when((role < 2) & jnp.logical_not(outer))
         def _():
-            to_inner(role, to).wait_recv()
-            to_peer[to] = (summed + merging[role].astype(jnp.float32)).astype(jnp.bfloat16)
-            to_place(role, to).start()
+            to_inner(role, to, h).wait_recv()
+            to_peer[slot] = (
+                summed + merging[role * PARTS + h].astype(jnp.float32)
+            ).astype(jnp.bfloat16)
+            to_place(role, to, h).start()
 
         @pl.when(role == 2)
         def _():
-            to_peer[to] = summed.astype(jnp.bfloat16)
-            to_pair().start()
+            to_peer[slot] = summed.astype(jnp.bfloat16)
+            to_pair(h).start()
 
         @pl.when(role == 3)
         def _():
-            final[...] = summed
+            final[h] = summed
 
         return carry
 
-    lax.fori_loop(0, places, compute, 0)
-
-    to_pair().wait_recv()
-    total = final[...] + from_peer[1].astype(jnp.float32)
-    to_place(0, z).wait_recv()
-    out_ref[...] = (total + from_peer[0].astype(jnp.float32)).astype(out_ref.dtype)
+    lax.fori_loop(0, places * PARTS, compute, 0)
+
+    for h in range(PARTS):
+        to_pair(h).wait_recv()
+        total = final[h] + from_peer[PARTS + h].astype(jnp.float32)
+        to_place(0, z, h).wait_recv()
+        out_ref[h * part_rows : (h + 1) * part_rows, :] = (
+            total + from_peer[h].astype(jnp.float32)
+        ).astype(out_ref.dtype)
 
     inward.drain()
     outward.drain()
@@ -709,19 +740,20 @@
 
                 share(places - 1 + k, z + k, c, p).wait_send()
 
-    for d in range(places):
-        to_sibling(d, d).wait_send()
-    for role, to in ((0, far), (1, near)):
-
-        @pl.when(outer)
-        def _():
-            to_inner(role, to).wait_send()
-
-        @pl.when(jnp.logical_not(outer))
-        def _():
-            to_place(role, to).wait_send()
-
-    to_pair().wait_send()
+    for step in range(places * PARTS):
+        to_sibling(step).wait_send()
+    for h in range(PARTS):
+        for role, to in ((0, far), (1, near)):
+
+            @pl.when(outer)
+            def _():
+                to_inner(role, to, h).wait_send()
+
+            @pl.when(jnp.logical_not(outer))
+            def _():
+                to_place(role, to, h).wait_send()
+
+        to_pair(h).wait_send()
 
 
 def fused(
@@ -757,8 +789,8 @@
             dma((count,)),
             dma((places, count)),
             dma((places, count)),
-            dma((2, places)),
-            dma((2, places)),
+            dma((2, 2 * places)),
+            dma((2, 2 * places)),
             dma((2, places)),
             dma((2, places)),
         ]
@@ -779,12 +811,12 @@
             pltpu.VMEM((length, GROUP_DIM), low),
             pltpu.VMEM((length, GROUP_DIM), low),
             pltpu.VMEM((length + 16, GROUP_DIM), low),
-            pltpu.VMEM((places, row_count, half_out), low),
-            pltpu.VMEM((places, row_count, half_out), low),
-            pltpu.VMEM((places, row_count, half_out), low),
-            pltpu.VMEM((2, row_count, half_out), low),
-            pltpu.VMEM((2, row_count, half_out), low),
-            pltpu.VMEM((row_count, half_out), jnp.float32),
+            pltpu.VMEM((places * PARTS, row_count // PARTS, half_out), low),
+            pltpu.VMEM((places * PARTS, row_count // PARTS, half_out), low),
+            pltpu.VMEM((places * PARTS, row_count // PARTS, half_out), low),
+            pltpu.VMEM((2 * PARTS, row_count // PARTS, half_out), low),
+            pltpu.VMEM((2 * PARTS, row_count // PARTS, half_out), low),
+            pltpu.VMEM((PARTS, row_count // PARTS, half_out), jnp.float32),
             dma,
             *gather_sems(4),
             *gather_sems(2),
@@ -794,12 +826,12 @@
             dma((places + 1, PIECES)),
             dma((2 * places, PIECES)),
             dma((2 * places, PIECES)),
-            dma((places,)),
-            dma((places,)),
-            dma((3,)),
-            dma((2,)),
-            dma((2,)),
-            dma((2,)),
+            dma((places * PARTS,)),
+            dma((places * PARTS,)),
+            dma((3 * PARTS,)),
+            dma((2 * PARTS,)),
+            dma((2 * PARTS,)),
+            dma((2 * PARTS,)),
         ],
         compiler_params=pltpu.CompilerParams(
             collective_id=0, has_side_effects=True, vmem_limit_bytes=56 * 1024 * 1024

time: 127 us -> 127 us (level)
  no operation moved by 1% of the time
where the time goes in v4:
time: 127 us; the launch traced here: 126 us
  Pallas kernels  124 us (98%)
  local copies, waits for them, and re-layouts  1.87 us (1%)
    pallas_call x1, Pallas kernels, fused(): pl.pallas_call(lambda *refs: fused_kernel(places, groups, *refs), out_sha...  124 us

profile of v4, /device:TPU:10, one launch (start us, length us, event | category | flops | bytes accessed | tf_op | source)
XLA Modules:
  0.0 126.4 jit_solution(15792883224216550993)
XLA Ops:
  0.0 0.6 maximum_bitcast_fusion.refs_2_
  0.6 123.9 %shard_map.118 = bf16[256,1024]{1,0:T(8,128)(2,1)} custom-call(bf16[256,2048]{1,0:T(8,128)(2,1)} %bitcast.8, f32[1,2048]{1,0:T(1,128)} %bitcast.9, f32[1,128]{1,0:T(1,128)} %maximum_bitcast_fusion.refs_2_, bf16[128,1024]{1,0:T(8,128)(2,1)} %refs_3_.1, bf16[128,1024]{1,0:T(8,128)(2,1)} %refs_4_.1, bf16[128,1024]{1,0:T(8,128)(2,1)} %refs_5_.1, ...), custom_call_target="tpu_custom_call" | custom-call | tf_op jit(solution)/shard_map/pallas_call | solution.py:798
  124.6 1.9 %copy.14 = bf16[1,256,1024]{2,1,0:T(8,128)(2,1)} copy(bf16[1,256,1024]{2,1,0:T(8,128)(2,1)} %bitcast.7) | data formatting | bytes 1048576
  (1 shorter events, 0.0 us)

commit v5 on v4

--- a/solution.py
+++ b/solution.py
@@ -225,6 +225,8 @@
     from_peer,
     merging,
     final,
+    pooled_all,
+    attn_all,
     *sems,
 ):
     (
@@ -352,16 +354,18 @@
                 {"fs": (fx, fy)[side]},
             )
 
-        def start(self):
+        def start_own(self):
             for m in range(self.count):
                 self.own(m).start()
+
+        def start(self):
             for d in range(1, places):
                 for m in range(self.count):
                     self.across(d, m).start()
 
         def first(self, d):
             for m in range(self.count):
-                if d == 0:
+                if isinstance(d, int) and d == 0:
                     self.own(m).wait()
                 else:
                     self.arrive(d, m).wait_recv()
@@ -434,8 +438,9 @@
     own_rows = pltpu.make_async_copy(
         normed_ref, rows_all.at[block(2 * z + c, half_rows), :], own_sem
     )
+    inward.start_own()
     inward.start()
-    outward.start()
+    outward.start_own()
     floated = tokens_ref[pl.ds(pl.multiple_of(c * half_rows, 16), half_rows), :].astype(
         jnp.float32
     )
@@ -505,15 +510,11 @@
         inward.second(d - 1)
     outward.first(0)
     inward.second(places - 1)
-    for d in range(1, places):
-        outward.first(d)
-        if d > 1:
-            outward.second(d - 2)
-    tokens_step(1)
-    for d in (places - 2, places - 1):
-        outward.second(d)
-    for k in range(2, places):
+    for k in range(1, places - 1):
         tokens_step(k)
+    outward.start()
+    outward.second(0)
+    tokens_step(places - 1)
     for d in range(places):
         inward.third(d)
 
@@ -559,8 +560,6 @@
         return carry
 
     lax.fori_loop(0, places, project, 0)
-    for d in range(places):
-        outward.third(d)
 
     level = lax.rem(c * map_ref.shape[0] + z, 4)
     window = jnp.where(
@@ -569,58 +568,10 @@
     head_lambda = lambda_ref[c * map_ref.shape[0] + z]
     length = places * row_count
 
-    part_rows = row_count // PARTS
-
-    def to_sibling(step):
-        return remote(
-            to_mate.at[step],
-            from_mate.at[step],
-            half_send.at[step],
-            half_recv.at[step],
-            {"tp": mate},
-        )
-
-    outer = (z == 0) | (z == places - 1)
-    pair = z + 1 - 2 * lax.rem(z, 2)
-    far = jnp.where(z < 2, places - 1, 0)
-    near = jnp.where(z < 2, 2, 1)
-
-    def to_inner(role, to, h):
-        return remote(
-            to_peer.at[to * PARTS + h],
-            merging.at[role * PARTS + h],
-            merge_send.at[role * PARTS + h],
-            merge_recv.at[role * PARTS + h],
-            {"sp": pair},
-        )
-
-    def to_place(role, to, h):
-        return remote(
-            to_peer.at[to * PARTS + h],
-            from_peer.at[h],
-            peer_send.at[role * PARTS + h],
-            peer_recv.at[h],
-            {"sp": to},
-        )
-
-    def to_pair(h):
-        return remote(
-            to_peer.at[pair * PARTS + h],
-            from_peer.at[PARTS + h],
-            peer_send.at[2 * PARTS + h],
-            peer_recv.at[PARTS + h],
-            {"sp": pair},
-        )
-
-    def compute(step, carry):
-        turn = step // PARTS
-        h = lax.rem(step, PARTS)
-        role = jnp.where((turn == 3) | outer, turn, lax.rem(turn + 2, 3))
-        to = jnp.where(role == 0, far, jnp.where(role == 1, near, jnp.where(role == 2, pair, z)))
-        slot = to * PARTS + h
-        rows = block(slot, part_rows)
-        query_pos = slot * part_rows + lax.broadcasted_iota(jnp.int32, (part_rows, length), 0)
-        key_pos = lax.broadcasted_iota(jnp.int32, (part_rows, length), 1)
+    def attend(index, carry):
+        rows = block(index, row_count)
+        query_pos = index * row_count + lax.broadcasted_iota(jnp.int32, (row_count, length), 0)
+        key_pos = lax.broadcasted_iota(jnp.int32, (row_count, length), 1)
         seen = query_pos >= key_pos
         mapped = []
         for m in range(2):
@@ -648,19 +599,89 @@
             * HEAD_SCALE
         ).astype(jnp.bfloat16)
         extended = pools[
-            pl.ds(pl.multiple_of(slot * part_rows, 16), part_rows + 16), :
+            pl.ds(pl.multiple_of(index * row_count, 16), row_count + 16), :
         ].astype(jnp.float32)
         picked = extended + pltpu.roll(extended, 1, 0)
         sums = picked
         for shift in (2, 4, 8):
             sums = sums + pltpu.roll(sums, shift, 0)
             picked = lax.select_n(window >= 2 * shift, picked, sums)
-        places_of = slot * part_rows + lax.broadcasted_iota(jnp.int32, (part_rows, 1), 0)
+        places_of = index * row_count + lax.broadcasted_iota(jnp.int32, (row_count, 1), 0)
         counts = jnp.minimum(places_of + 1, window).astype(jnp.float32)
         mixed = (picked[16:] / counts - extended[16:]).astype(jnp.bfloat16)
         pooled = (
             jnp.dot(mixed, map_ref[z], preferred_element_type=jnp.float32) * scale_ref[z]
         ).astype(jnp.bfloat16)
+        pooled_all[rows, :] = pooled
+        attn_all[rows, :] = attn
+
+        @pl.when(index < places - 1)
+        def _():
+            outward.first(index + 1)
+
+        @pl.when((index > 0) & (index < places - 1))
+        def _():
+            outward.second(index)
+
+        return carry
+
+    lax.fori_loop(0, places, attend, 0)
+    outward.second(places - 1)
+    for d in range(places):
+        outward.third(d)
+
+    part_rows = row_count // PARTS
+
+    def to_sibling(step):
+        return remote(
+            to_mate.at[step],
+            from_mate.at[step],
+            half_send.at[step],
+            half_recv.at[step],
+            {"tp": mate},
+        )
+
+    outer = (z == 0) | (z == places - 1)
+    pair = z + 1 - 2 * lax.rem(z, 2)
+    far = jnp.where(z < 2, places - 1, 0)
+    near = jnp.where(z < 2, 2, 1)
+
+    def to_inner(role, to, h):
+        return remote(
+            to_peer.at[to * PARTS + h],
+            merging.at[role * PARTS + h],
+            merge_send.at[role * PARTS + h],
+            merge_recv.at[role * PARTS + h],
+            {"sp": pair},
+        )
+
+    def to_place(role, to, h):
+        return remote(
+            to_peer.at[to * PARTS + h],
+            from_peer.at[h],
+            peer_send.at[role * PARTS + h],
+            peer_recv.at[h],
+            {"sp": to},
+        )
+
+    def to_pair(h):
+        return remote(
+            to_peer.at[pair * PARTS + h],
+            from_peer.at[PARTS + h],
+            peer_send.at[2 * PARTS + h],
+            peer_recv.at[PARTS + h],
+            {"sp": pair},
+        )
+
+    def compute(step, carry):
+        turn = step // PARTS
+        h = lax.rem(step, PARTS)
+        role = jnp.where((turn == 3) | outer, turn, lax.rem(turn + 2, 3))
+        to = jnp.where(role == 0, far, jnp.where(role == 1, near, jnp.where(role == 2, pair, z)))
+        slot = to * PARTS + h
+        rows = block(slot, part_rows)
+        pooled = pooled_all[rows, :]
+        attn = attn_all[rows, :]
 
         def partial_of(side):
             columns = block(side, half_out)
@@ -817,6 +838,8 @@
             pltpu.VMEM((2 * PARTS, row_count // PARTS, half_out), low),
             pltpu.VMEM((2 * PARTS, row_count // PARTS, half_out), low),
             pltpu.VMEM((PARTS, row_count // PARTS, half_out), jnp.float32),
+            pltpu.VMEM((length, GROUP_DIM), low),
+            pltpu.VMEM((length, GROUP_DIM), low),
             dma,
             *gather_sems(4),
             *gather_sems(2),

time: 127 us -> 133 us (1.047)
  the two profiles are of different devices: /device:TPU:10 before, /device:TPU:16 now
where the time goes in v5:
time: 133 us
  Pallas kernels  130 us (98%)
  local copies, waits for them, and re-layouts  1.87 us (1%)
    pallas_call x1, Pallas kernels, fused(): pl.pallas_call(lambda *refs: fused_kernel(places, groups, *refs), out_sha...  130 us

profile of v5, /device:TPU:16, one launch (start us, length us, event | category | flops | bytes accessed | tf_op | source)
XLA Modules:
  0.0 132.6 jit_solution(59058021706242108)
XLA Ops:
  0.0 0.6 maximum_bitcast_fusion.refs_2_
  0.6 130.1 %shard_map.118 = bf16[256,1024]{1,0:T(8,128)(2,1)} custom-call(bf16[256,2048]{1,0:T(8,128)(2,1)} %bitcast.8, f32[1,2048]{1,0:T(1,128)} %bitcast.9, f32[1,128]{1,0:T(1,128)} %maximum_bitcast_fusion.refs_2_, bf16[128,1024]{1,0:T(8,128)(2,1)} %refs_3_.1, bf16[128,1024]{1,0:T(8,128)(2,1)} %refs_4_.1, bf16[128,1024]{1,0:T(8,128)(2,1)} %refs_5_.1, ...), custom_call_target="tpu_custom_call" | custom-call | tf_op jit(solution)/shard_map/pallas_call | solution.py:819
  130.7 1.9 %copy.14 = bf16[1,256,1024]{2,1,0:T(8,128)(2,1)} copy(bf16[1,256,1024]{2,1,0:T(8,128)(2,1)} %bitcast.7) | data formatting | bytes 1048576
  (1 shorter events, 0.0 us)
